TPU v7x, 32 devices: a whole 2x2x4 slice. The times are simulated.
32 devices in a mesh: grp: 2 (over x), sp: 4 (over y, core), tp: 4 (over z).
Axes of the slice: x: 2, y: 2, z: 4, core: 2. Of those that a mesh axis runs over, the one named last changes fastest.
Arguments:
- residual: bfloat16 [768, 8, 2048], P(('sp', 'tp'), 'grp'), parts along dimension 1, may hold values from -6 to 6
- query: bfloat16 [768, 8, 1536], P('sp', 'grp', 'tp'), parts along dimension 1, may hold values from -64 to 64
- latent: bfloat16 [768, 8, 512], P('sp', 'grp'), parts along dimension 1, may hold values from -6 to 6
- rope_key: bfloat16 [768, 8, 64], P('sp', 'grp'), parts along dimension 1, may hold values from -8 to 8
- latent_gain: float32 [512], replicated, may hold values from 0.1 to 1.9
- key_up: bfloat16 [512, 1024], P(None, 'tp'), may hold values from -0.25 to 0.25
- value_up: bfloat16 [512, 1024], P(None, 'tp'), may hold values from -0.25 to 0.25
- out_weight: bfloat16 [1024, 2048], P('tp'), may hold values from -0.375 to 0.375
- norm_gain: float32 [2048], replicated, may hold values from 0.1 to 1.9
- group_prob: float32 [768, 8], P(('sp', 'tp'), 'grp'), parts along dimension 1, may hold values from 0.25 to 1
- pair_logits: float32 [768, 8, 2], P(('sp', 'tp'), 'grp'), parts along dimension 1, may hold values from -8 to 8
- routes: int32 [768, 8, 2], P(('sp', 'tp'), 'grp'), parts along dimension 1, may hold values from 0 to 15, all different within a row; in each aligned block of 192 rows (0 to 191, 192 to 383, ..., all dimensions but the last counted through in order) at most 36 rows name the same one
- w_gate: bfloat16 [16, 2048, 768], P(('sp', 'tp')), may hold values from -0.125 to 0.125
- w_up: bfloat16 [16, 2048, 768], P(('sp', 'tp')), may hold values from -0.125 to 0.125
- w_down: bfloat16 [16, 768, 2048], P(('sp', 'tp')), may hold values from -0.4375 to 0.4375
Outputs:
- layer_out: bfloat16 [768, 8, 2048], P(('sp', 'tp'), 'grp'), parts along dimension 1
There are 2 independent parts, one for each index of `grp`. A program takes and returns all parts, laid end to end along the dimension named above; an argument that names none is the same for every part. Nothing has to cross between parts.
Inputs may be any that keep to these rules, and one draw needn't show every extreme that they name: `routes`: A token's 2 experts differ. Among the tokens of one device (aligned blocks of 192 rows in position-then-sequence order), no expert is named more than 36 times, a bound that some block reaches.
All inputs are finite; a program needn't handle non-finite values.
Results may differ from a plain program's by a relative error of at most 0.013.
Values may be sent and summed in bfloat16 or wider, within the bound.
A program may use at most 128 MiB of HBM per device.

v0:
```python
import jax
import jax.numpy as jnp
from jax import lax
from jax.sharding import PartitionSpec as P

D = 2048
NOPE = 128
VDIM = 128
QK = 192
TOPK = 2
SEQS = 4


epsilon = 1e-06
rotary_base = 10000.0
lowest = -1e30


def rotate(values, positions):
    halfway = values.shape[-1] // 2
    inverse = rotary_base ** (-jnp.arange(halfway, dtype=jnp.float32) / halfway)
    angles = positions.astype(jnp.float32)[:, None] * inverse[None, :]
    angles = angles.reshape((angles.shape[0],) + (1,) * (values.ndim - 2) + (halfway,))
    cosine_values = jnp.cos(angles)
    sine_values = jnp.sin(angles)
    first_half = values[..., :halfway]
    second_half = values[..., halfway:]
    return jnp.concatenate(
        [
            first_half * cosine_values - second_half * sine_values,
            second_half * cosine_values + first_half * sine_values,
        ],
        axis=-1,
    )


def rms_scale(values, gain_values):
    return (
        values
        * lax.rsqrt(jnp.mean(values * values, axis=-1, keepdims=True) + epsilon)
        * gain_values
    )


def expand(latent_rows, latent_gain, key_up, value_up):
    normed = rms_scale(latent_rows.astype(jnp.float32), latent_gain).astype(jnp.bfloat16)
    keys_nope = jnp.dot(normed, key_up, preferred_element_type=jnp.float32).astype(jnp.bfloat16)
    values = jnp.dot(normed, value_up, preferred_element_type=jnp.float32).astype(jnp.bfloat16)
    lead = latent_rows.shape[:2]
    return (
        keys_nope.reshape(lead + (key_up.shape[1] // NOPE, NOPE)),
        values.reshape(lead + (value_up.shape[1] // VDIM, VDIM)),
    )


def absorb(carried, query_nope, query_rot, key_nope, value_rows, key_rot):
    running, totals, accumulated = carried
    scores = jnp.einsum("qshd,kshd->qshk", query_nope, key_nope, preferred_element_type=jnp.float32)
    scores = scores + jnp.einsum(
        "qshd,ksd->qshk", query_rot, key_rot, preferred_element_type=jnp.float32
    )
    scores = scores * QK ** (-0.5)
    highest = jnp.maximum(running, jnp.max(scores, axis=-1))
    weights = jnp.exp(scores - highest[..., None])
    totals = jnp.sum(weights, axis=-1)
    accumulated = jnp.einsum(
        "qshk,kshd->qshd",
        weights.astype(jnp.bfloat16),
        value_rows,
        preferred_element_type=jnp.float32,
    )
    return (highest, totals, accumulated)


def shards(
    residual,
    query,
    latent,
    rope_key,
    latent_gain,
    key_up,
    value_up,
    out_weight,
    norm_gain,
    group_prob,
    pair_logits,
    routes,
    w_gate,
    w_up,
    w_down,
):
    positions_here = query.shape[0]
    heads_here = key_up.shape[1] // NOPE
    own_positions = lax.axis_index("sp") * positions_here + jnp.arange(
        positions_here, dtype=jnp.int32
    )
    split_query = query.reshape(positions_here, SEQS, heads_here, QK)
    query_nope = split_query[..., :NOPE]
    query_rot = rotate(split_query[..., NOPE:].astype(jnp.float32), own_positions).astype(
        jnp.bfloat16
    )
    key_rot = rotate(rope_key.astype(jnp.float32), own_positions).astype(jnp.bfloat16)
    initial = (
        jnp.full((positions_here, SEQS, heads_here), lowest, jnp.float32),
        jnp.zeros((positions_here, SEQS, heads_here), jnp.float32),
        jnp.zeros((positions_here, SEQS, heads_here, VDIM), jnp.float32),
    )
    key_nope, value_rows = expand(
        lax.all_gather(latent, "sp", axis=0, tiled=True), latent_gain, key_up, value_up
    )
    finished = absorb(
        initial,
        query_nope,
        query_rot,
        key_nope,
        value_rows,
        lax.all_gather(key_rot, "sp", axis=0, tiled=True),
    )
    attended = (finished[2] / finished[1][..., None]).astype(jnp.bfloat16)
    attended = attended.reshape(positions_here, SEQS, heads_here * VDIM)
    by_token = lax.all_to_all(attended, "tp", split_axis=0, concat_axis=2, tiled=True)
    row_count = by_token.shape[0] * SEQS
    mixed_heads = by_token.reshape(row_count, by_token.shape[2])
    projected = jnp.dot(
        mixed_heads,
        lax.all_gather(out_weight, "tp", axis=0, tiled=True),
        preferred_element_type=jnp.float32,
    )
    stream = (residual.reshape(row_count, D).astype(jnp.float32) + projected).astype(jnp.bfloat16)
    normed = rms_scale(stream.astype(jnp.float32), norm_gain).astype(jnp.bfloat16)
    mixing = jax.nn.softmax(pair_logits.reshape(row_count, TOPK), axis=-1) * group_prob.reshape(
        row_count, 1
    )
    experts_total = lax.axis_size("sp") * lax.axis_size("tp")
    capacity = max(2, 3 * row_count * TOPK // (2 * experts_total))
    pick_count = row_count * TOPK
    chosen = routes.reshape(pick_count)
    one_hot = (chosen[:, None] == jnp.arange(experts_total, dtype=jnp.int32)[None, :]).astype(
        jnp.bfloat16
    )
    earlier = (jnp.arange(pick_count)[:, None] > jnp.arange(pick_count)[None, :]).astype(
        jnp.bfloat16
    )
    before = jnp.dot(earlier, one_hot, preferred_element_type=jnp.float32)
    slot_index = jnp.sum(before * one_hot.astype(jnp.float32), axis=-1).astype(jnp.int32)
    target = chosen * capacity + slot_index
    source_row = (
        jnp.full((experts_total * capacity,), row_count, jnp.int32)
        .at[target]
        .set(jnp.arange(pick_count, dtype=jnp.int32) // TOPK)
    )
    padded = jnp.concatenate([normed, jnp.zeros((1, D), jnp.bfloat16)], axis=0)
    outgoing = padded[source_row].reshape(experts_total, capacity, D)
    arrived = lax.all_to_all(outgoing, ("sp", "tp"), split_axis=0, concat_axis=0, tiled=True)
    flat_rows = arrived.reshape(-1, D)
    gate_pre = jnp.dot(flat_rows, w_gate[0], preferred_element_type=jnp.float32)
    upward = jnp.dot(flat_rows, w_up[0], preferred_element_type=jnp.float32)
    hidden = (jax.nn.silu(gate_pre) * upward).astype(jnp.bfloat16)
    served = (
        jnp.dot(hidden, w_down[0], preferred_element_type=jnp.float32)
        .astype(jnp.bfloat16)
        .reshape(arrived.shape)
    )
    returned = lax.all_to_all(served, ("sp", "tp"), split_axis=0, concat_axis=0, tiled=True)
    results = returned.reshape(experts_total * capacity, D)[target].reshape(row_count, TOPK, D)
    combined = stream.astype(jnp.float32) + jnp.sum(
        results.astype(jnp.float32) * mixing[..., None], axis=1
    )
    return combined.astype(jnp.bfloat16).reshape(residual.shape)


def solution(mesh):
    placed = (
        P(("sp", "tp"), "grp", None),
        P("sp", "grp", "tp"),
        P("sp", "grp", None),
        P("sp", "grp", None),
        P(),
        P(None, "tp"),
        P(None, "tp"),
        P("tp", None),
        P(),
        P(("sp", "tp"), "grp"),
        P(("sp", "tp"), "grp", None),
        P(("sp", "tp"), "grp", None),
        P(("sp", "tp"), None, None),
        P(("sp", "tp"), None, None),
        P(("sp", "tp"), None, None),
    )
    return jax.shard_map(
        shards, mesh=mesh, in_specs=placed, out_specs=P(("sp", "tp"), "grp", None), check_vma=False
    )
```

profile of v0, /device:TPU:0, one launch (start us, length us, event | category | flops | bytes accessed | tf_op | source)
XLA Modules:
  0.0 339.8 jit_solution(12813253830816138456)
XLA Ops:
  8.0 1.9 copy.68
  10.0 3.2 reshape.281
  15.5 1.8 convert_element_type.93
  17.2 1.8 copy.71
  20.8 1.5 copy.73
  22.3 1.5 copy.72
  25.6 1.4 subtract_convert_fusion
  27.3 15.0 %all_gather.10 = bf16[768,4,64]{2,1,0:T(4,128)(2,1)} all-gather(bf16[192,4,64]{2,1,0:T(4,128)(2,1)S(1)} %pad_maximum_fusion), channel_id=1, replica_groups=mesh['grp'=2,'sp'=4,'tp'=4] {'sp'}, dimensions={0}, use_global_device_ids=true | all-gather | bytes 491520 | tf_op jit(solution)/shard_map/all_gather | solution.py:117
  44.4 3.0 fusion
  47.4 3.2 fusion.27
  52.7 1.3 fusion.4
  54.0 2.2 fusion.24
  58.9 4.6 %all-to-all-start = ((bf16[192,4,256]{2,1,0:T(4,128)(2,1)}), bf16[192,4,256]{2,1,0:T(4,128)(2,1)S(1)}, u32[]{:S(2)}, u32[]{:S(2)}) async-start(bf16[192,4,256]{2,1,0:T(4,128)(2,1)} %reshape.320), calls=%async_computation | async-start | bytes 786432 | tf_op jit(solution)/shard_map/all_to_all | solution.py:121
  63.7 2.5 reshape.290
  68.1 2.9 scatter_custom_fusion
  71.0 15.3 %all-to-all-done = bf16[192,4,256]{2,1,0:T(4,128)(2,1)S(1)} async-done(((bf16[192,4,256]{2,1,0:T(4,128)(2,1)}), bf16[192,4,256]{2,1,0:T(4,128)(2,1)S(1)}, u32[]{:S(2)}, u32[]{:S(2)}) %all-to-all-start) | async-done | bytes 393248 | tf_op jit(solution)/shard_map/all_to_all | solution.py:121
  86.7 48.3 %all-gather.5.cloned.1.call-done = bf16[1024,2048]{1,0:T(8,128)(2,1)} async-done(((bf16[256,2048]{1,0:T(8,128)(2,1)}), bf16[1024,2048]{1,0:T(8,128)(2,1)}) %all-gather.5.cloned.1.call-update) | async-done | bytes 4194320 | tf_op jit(solution)/shard_map/all_gather | solution.py:126
  135.0 3.8 %multiply_reduce_fusion.1 = (f32[192]{0:T(256)S(1)}, f32[192,2048]{1,0:T(8,128)S(1)}) fusion(f32[192,2048]{1,0:T(8,128)} %reshape.290, bf16[192,1024]{1,0:T(8,128)(2,1)S(1)} %bitcast.53, bf16[1024,2048]{1,0:T(8,128)(2,1)} %all-gather.5.cloned.1.call-done), kind=kOutput, calls=%fused_computation.33 | convolution fusion | flops 807272256 | bytes 7734016 | tf_op jit(solution)/shard_map/dot_general | solution.py:124
  141.2 8.1 %gather_fusion = bf16[576,2048]{1,0:T(8,128)(2,1)} fusion(bf16[193,2048]{1,0:T(8,128)(2,1)} %concatenate.13, s32[1024]{0:T(1024)S(1)} %pad_clamp_fusion.1), kind=kCustom, calls=%fused_computation | custom fusion | bytes 4720896 | tf_op jit(solution)/shard_map/gather | solution.py:153
  149.3 4.1 %reshape.284 = bf16[16,36,2048]{2,1,0:T(8,128)(2,1)} reshape(bf16[576,2048]{1,0:T(8,128)(2,1)} %gather_fusion) | data formatting | bytes 4718592 | tf_op jit(solution)/shard_map/reshape | solution.py:153
  153.3 65.1 %all_to_all.25 = bf16[16,36,2048]{2,1,0:T(8,128)(2,1)} all-to-all(bf16[16,36,2048]{2,1,0:T(8,128)(2,1)} %reshape.284), channel_id=1, replica_groups=mesh['grp'=2,'sp'=4,'tp'=4] {'sp','tp'}, dimensions={0} | all-to-all | bytes 4718592 | tf_op jit(solution)/shard_map/all_to_all | solution.py:154
  218.4 4.1 %reshape.285 = bf16[576,2048]{1,0:T(8,128)(2,1)} reshape(bf16[16,36,2048]{2,1,0:T(8,128)(2,1)} %all_to_all.25) | data formatting | bytes 4718592 | tf_op jit(solution)/shard_map/reshape | solution.py:155
  222.5 5.8 %fusion.10 = f32[576,768]{1,0:T(8,128)} fusion(bf16[576,2048]{1,0:T(8,128)(2,1)} %reshape.285, bf16[1,2048,768]{2,1,0:T(8,128)(2,1)} %param.27), kind=kOutput, calls=%fused_computation.17 | convolution fusion | flops 1811939328 | bytes 7274496 | tf_op jit(solution)/shard_map/dot_general | solution.py:156
  228.3 8.9 %fusion.12 = bf16[576,2048]{1,0:T(8,128)(2,1)} fusion(bf16[1,768,2048]{2,1,0:T(8,128)(2,1)S(1)} %copy-done, f32[576,768]{1,0:T(8,128)} %fusion.10, bf16[576,2048]{1,0:T(8,128)(2,1)} %reshape.285, bf16[1,2048,768]{2,1,0:T(8,128)(2,1)} %param.28), kind=kOutput, calls=%fused_computation.20 | convolution fusion | flops 3627712512 | bytes 12779520 | tf_op jit(solution)/shard_map/dot_general | solution.py:160
  237.2 4.1 %reshape.286 = bf16[16,36,2048]{2,1,0:T(8,128)(2,1)} reshape(bf16[576,2048]{1,0:T(8,128)(2,1)} %fusion.12) | data formatting | bytes 4718592 | tf_op jit(solution)/shard_map/reshape | solution.py:162
  241.4 4.8 %all-to-all-start.2 = ((bf16[16,36,2048]{2,1,0:T(8,128)(2,1)}), bf16[16,36,2048]{2,1,0:T(8,128)(2,1)}, u32[]{:S(2)}, u32[]{:S(2)}) async-start(bf16[16,36,2048]{2,1,0:T(8,128)(2,1)} %reshape.286), calls=%async_computation.2 | async-start | bytes 5242880 | tf_op jit(solution)/shard_map/all_to_all | solution.py:164
  247.2 59.3 %all-to-all-done.2 = bf16[16,36,2048]{2,1,0:T(8,128)(2,1)} async-done(((bf16[16,36,2048]{2,1,0:T(8,128)(2,1)}), bf16[16,36,2048]{2,1,0:T(8,128)(2,1)}, u32[]{:S(2)}, u32[]{:S(2)}) %all-to-all-start.2) | async-done | bytes 2359328 | tf_op jit(solution)/shard_map/all_to_all | solution.py:164
  306.6 4.1 %reshape.287 = bf16[576,2048]{1,0:T(8,128)(2,1)} reshape(bf16[16,36,2048]{2,1,0:T(8,128)(2,1)} %all-to-all-done.2) | data formatting | bytes 4718592 | tf_op jit(solution)/shard_map/reshape | solution.py:165
  310.7 7.0 %gather_fusion.1 = bf16[384,2048]{1,0:T(8,128)(2,1)} fusion(bf16[576,2048]{1,0:T(8,128)(2,1)} %reshape.287, s32[1024]{0:T(1024)S(1)} %pad_clamp_fusion), kind=kCustom, calls=%fused_computation.1 | custom fusion | bytes 3147264 | tf_op jit(solution)/shard_map/gather | solution.py:165
  317.7 4.8 %reshape.291 = f32[192,2,2048]{2,1,0:T(2,128)} reshape(bf16[384,2048]{1,0:T(8,128)(2,1)} %gather_fusion.1) | data formatting | bytes 4718592 | tf_op jit(solution)/shard_map/convert_element_type | solution.py:167
  322.5 7.0 %multiply_reduce_fusion = f32[192,2048]{1,0:T(8,128)S(1)} fusion(f32[192,2,2048]{2,1,0:T(2,128)} %reshape.291, f32[192,2]{1,0:T(8,128)S(1)} %copy.86), kind=kLoop, calls=%fused_computation.19 | loop fusion | flops 1179648 | bytes 4720128 | tf_op jit(solution)/shard_map/reduce_sum | solution.py:166
  330.5 2.4 reshape.289
  (76 shorter events, 21.3 us)
Async XLA Ops:
  6.5 221.8 %copy-start = (bf16[1,768,2048]{2,1,0:T(8,128)(2,1)S(1)}, bf16[1,768,2048]{2,1,0:T(8,128)(2,1)}, u32[]{:S(2)}) copy-start(bf16[1,768,2048]{2,1,0:T(8,128)(2,1)} %param.29) | copy-start | bytes 9437188
  6.5 37.8 %all-gather.3.cloned.1.call-start = ((), (), s32[]{:S(2)}) async-start(), calls=%async_computation.3 | async-start | bytes 3932160 | tf_op jit(solution)/shard_map/all_gather | solution.py:109
  7.3 127.7 %all-gather.5.cloned.1.call-start = ((), (), s32[]{:S(2)}) async-start(), calls=%async_computation.4 | async-start | bytes 5242880 | tf_op jit(solution)/shard_map/all_gather | solution.py:126
  8.0 15.8 %copy-start.7 = (s32[48,4,2]{0,2,1:T(2,128)S(1)}, s32[48,4,2]{0,2,1:T(2,128)}, u32[]{:S(2)}) copy-start(s32[48,4,2]{0,2,1:T(2,128)} %param.26) | copy-start | bytes 4612
  25.6 16.6 %copy-start.5 = (f32[192,4,2,64]{0,3,2,1:T(8,128)S(1)}, f32[192,4,2,64]{0,3,2,1:T(8,128)}, u32[]{:S(2)}) copy-start(f32[192,4,2,64]{0,3,2,1:T(8,128)} %convert_element_type.93) | copy-start | bytes 1179652
  27.0 20.3 %copy-start.11 = (f32[512]{0:T(512)S(1)}, f32[512]{0:T(512)}, u32[]{:S(2)}) copy-start(f32[512]{0:T(512)} %param.19) | copy-start | bytes 6148
  44.4 3.0 copy-start.3
  47.4 3.2 slice-start
  50.6 1.1 copy-start.4
  52.7 1.3 copy-start.10
  58.9 27.4 %all-to-all-start = ((bf16[192,4,256]{2,1,0:T(4,128)(2,1)}), bf16[192,4,256]{2,1,0:T(4,128)(2,1)S(1)}, u32[]{:S(2)}, u32[]{:S(2)}) async-start(bf16[192,4,256]{2,1,0:T(4,128)(2,1)} %reshape.320), calls=%async_computation | async-start | bytes 786432 | tf_op jit(solution)/shard_map/all_to_all | solution.py:121
  135.0 5.0 %copy-start.8 = (f32[2048]{0:T(1024)S(1)}, f32[2048]{0:T(1024)}, u32[]{:S(2)}) copy-start(f32[2048]{0:T(1024)} %param.23) | copy-start | bytes 24580
  138.8 1.2 copy-start.1
  241.4 4.8 %copy-start.6 = (f32[48,4,2]{0,2,1:T(2,128)S(1)}, f32[48,4,2]{0,2,1:T(2,128)}, u32[]{:S(2)}) copy-start(f32[48,4,2]{0,2,1:T(2,128)} %param.25) | copy-start | bytes 4612
  241.4 5.0 %copy-start.9 = (f32[48,4]{0,1:T(4,128)S(1)}, f32[48,4]{0,1:T(4,128)}, u32[]{:S(2)}) copy-start(f32[48,4]{0,1:T(4,128)} %param.24) | copy-start | bytes 2308
  241.4 65.2 %all-to-all-start.2 = ((bf16[16,36,2048]{2,1,0:T(8,128)(2,1)}), bf16[16,36,2048]{2,1,0:T(8,128)(2,1)}, u32[]{:S(2)}, u32[]{:S(2)}) async-start(bf16[16,36,2048]{2,1,0:T(8,128)(2,1)} %reshape.286), calls=%async_computation.2 | async-start | bytes 5242880 | tf_op jit(solution)/shard_map/all_to_all | solution.py:164
  322.5 7.0 %copy-start.2 = (f32[192,2048]{1,0:T(8,128)S(1)}, f32[192,2048]{1,0:T(8,128)}, u32[]{:S(2)}) copy-start(f32[192,2048]{1,0:T(8,128)} %copy-done.1) | copy-start | bytes 4718596
Sparse Core Ops, SparseCore 0:
  8.9 35.4 all-gather.2
  45.9 89.0 all-gather.4
where the time goes:
time: 341 us; the launch traced here: 340 us
  waiting for transfers between devices  126 us (37%)
  blocking collectives  80 us (23%)
  local copies, waits for them, and re-layouts  65.1 us (19%)
  matrix products  27.1 us (8%)
  other arithmetic  18.7 us (5%)
  between operations  13.7 us (4%)
  starting transfers between devices  9.45 us (3%)
    all_to_all x1, blocking collectives, shards(): lax.all_to_all(outgoing, ('sp', 'tp'), split_axis=0, concat_axis=0, tiled...  65.1 us
    all_to_all x1, waiting for transfers between devices, shards(): lax.all_to_all(served, ('sp', 'tp'), split_axis=0, concat_axis=0, tiled=T...  59.3 us
    all_gather x1, waiting for transfers between devices, shards(): lax.all_gather(out_weight, 'tp', axis=0, tiled=True)  48.3 us
    all_to_all x1, waiting for transfers between devices, shards(): lax.all_to_all(attended, 'tp', split_axis=0, concat_axis=2, tiled=True)  15.3 us
    all_gather x1, blocking collectives, shards(): lax.all_gather(key_rot, 'sp', axis=0, tiled=True)  15 us
    dot_general x1, matrix products, shards(): jnp.dot(hidden, w_down[0], preferred_element_type=jnp.float32)  8.94 us
    gather x1, local copies, waits for them, and re-layouts, shards(): outgoing = padded[source_row].reshape(experts_total, capacity, D)  8.09 us
    unnamed x31, local copies, waits for them, and re-layouts  7.23 us
  transfers between devices with their start and end apart: 4, of which 4 were waited for; matrix products, arithmetic and copies ran while one was open for 13% of the time, Pallas kernels for 0%

commit v1 on v0

--- a/solution.py
+++ b/solution.py
@@ -70,6 +70,26 @@
         preferred_element_type=jnp.float32,
     )
     return (highest, totals, accumulated)
+
+
+def slots(chosen, row_count, experts_total):
+    capacity = max(2, 3 * row_count * TOPK // (2 * experts_total))
+    capacity = -(-capacity // 8) * 8
+    one_hot = (chosen[:, None] == jnp.arange(experts_total, dtype=jnp.int32)[None, :]).astype(
+        jnp.bfloat16
+    )
+    order = jnp.arange(chosen.shape[0])
+    earlier = (order[:, None] > order[None, :]).astype(jnp.bfloat16)
+    before = jnp.dot(earlier, one_hot, preferred_element_type=jnp.float32)
+    slot_index = jnp.sum(before * one_hot.astype(jnp.float32), axis=-1).astype(jnp.int32)
+    return capacity, chosen * capacity + slot_index
+
+
+def whole_out_weight(out_weight):
+    pieces = lax.axis_size("sp")
+    depth = out_weight.shape[0] // pieces
+    own = lax.dynamic_slice_in_dim(out_weight, lax.axis_index("sp") * depth, depth, axis=0)
+    return lax.all_gather(own, ("tp", "sp"), axis=0, tiled=True)
 
 
 def shards(
@@ -123,7 +143,7 @@
     mixed_heads = by_token.reshape(row_count, by_token.shape[2])
     projected = jnp.dot(
         mixed_heads,
-        lax.all_gather(out_weight, "tp", axis=0, tiled=True),
+        whole_out_weight(out_weight),
         preferred_element_type=jnp.float32,
     )
     stream = (residual.reshape(row_count, D).astype(jnp.float32) + projected).astype(jnp.bfloat16)
@@ -132,25 +152,15 @@
         row_count, 1
     )
     experts_total = lax.axis_size("sp") * lax.axis_size("tp")
-    capacity = max(2, 3 * row_count * TOPK // (2 * experts_total))
-    pick_count = row_count * TOPK
-    chosen = routes.reshape(pick_count)
-    one_hot = (chosen[:, None] == jnp.arange(experts_total, dtype=jnp.int32)[None, :]).astype(
-        jnp.bfloat16
-    )
-    earlier = (jnp.arange(pick_count)[:, None] > jnp.arange(pick_count)[None, :]).astype(
-        jnp.bfloat16
-    )
-    before = jnp.dot(earlier, one_hot, preferred_element_type=jnp.float32)
-    slot_index = jnp.sum(before * one_hot.astype(jnp.float32), axis=-1).astype(jnp.int32)
-    target = chosen * capacity + slot_index
-    source_row = (
-        jnp.full((experts_total * capacity,), row_count, jnp.int32)
-        .at[target]
-        .set(jnp.arange(pick_count, dtype=jnp.int32) // TOPK)
-    )
-    padded = jnp.concatenate([normed, jnp.zeros((1, D), jnp.bfloat16)], axis=0)
-    outgoing = padded[source_row].reshape(experts_total, capacity, D)
+    capacity, target = slots(routes.reshape(row_count * TOPK), row_count, experts_total)
+    spots = target.reshape(row_count, TOPK)
+    places = jnp.arange(experts_total * capacity, dtype=jnp.int32)
+    picked = spots[:, :, None] == places[None, None, :]
+    pick_rows = jnp.any(picked, axis=1).astype(jnp.bfloat16)
+    outgoing = lax.dot_general(
+        pick_rows, normed, (((0,), (0,)), ((), ())), preferred_element_type=jnp.float32
+    ).astype(jnp.bfloat16)
+    outgoing = outgoing.reshape(experts_total, capacity, D)
     arrived = lax.all_to_all(outgoing, ("sp", "tp"), split_axis=0, concat_axis=0, tiled=True)
     flat_rows = arrived.reshape(-1, D)
     gate_pre = jnp.dot(flat_rows, w_gate[0], preferred_element_type=jnp.float32)
@@ -162,10 +172,12 @@
         .reshape(arrived.shape)
     )
     returned = lax.all_to_all(served, ("sp", "tp"), split_axis=0, concat_axis=0, tiled=True)
-    results = returned.reshape(experts_total * capacity, D)[target].reshape(row_count, TOPK, D)
-    combined = stream.astype(jnp.float32) + jnp.sum(
-        results.astype(jnp.float32) * mixing[..., None], axis=1
-    )
+    returned = returned.reshape(experts_total * capacity, D)
+    combined = stream.astype(jnp.float32)
+    for choice in range(TOPK):
+        combined = combined + mixing[:, choice, None] * jnp.dot(
+            picked[:, choice].astype(jnp.bfloat16), returned, preferred_element_type=jnp.float32
+        )
     return combined.astype(jnp.bfloat16).reshape(residual.shape)
 
 

time: 341 us -> 264 us (0.77)
  waiting for transfers between devices: 126 us -> 88 us
  local copies, waits for them, and re-layouts: 65.1 us -> 28.6 us
  other arithmetic: 18.7 us -> 11.4 us
  matrix products: 27.1 us -> 33 us
    all_gather x1, waiting for transfers between devices: 48.3 us -> 21.5 us  [whole_out_weight(): return lax.all_gather(own, ('tp', 'sp'), axis=0, tiled=True)]
    reshape x4 -> x0, local copies, waits for them, and re-layouts: 16.4 us -> none  [the longest x1 4.14 us: shards(): served = jnp.dot(hidden, w_down[0], preferred_element_type=jnp.float32).a...]
    gather x2 -> x0, local copies, waits for them, and re-layouts: 15.1 us -> none  [the longest x1 8.09 us: shards(): outgoing = padded[source_row].reshape(experts_total, capacity, D)]
    all_to_all x1, waiting for transfers between devices: 15.3 us -> 3.55 us  [shards(): lax.all_to_all(attended, 'tp', split_axis=0, concat_axis=2, tiled=True)]
    dot_general x2 -> x5, matrix products: 3.99 us -> 11.5 us  [the longest x2 6.52 us: shards(): jnp.dot(picked[:, choice].astype(jnp.bfloat16), returned, preferred_eleme...]
    reduce_sum x1 -> x0, other arithmetic: 6.96 us -> none  [shards(): jnp.sum(results.astype(jnp.float32) * mixing[..., None], axis=1)]
    unnamed x31 -> x41, local copies, waits for them, and re-layouts: 7.23 us -> 7.63 us
  transfers between devices with their start and end apart: 4 -> 4, of which waited for: 4 -> 4; matrix products, arithmetic and copies ran while one was open for 13% -> 17% of each run, Pallas kernels for 0% -> 0%
where the time goes in v1:
time: 264 us; the launch traced here: 263 us
  waiting for transfers between devices  88 us (33%)
  blocking collectives  78.8 us (30%)
  matrix products  33 us (12%)
  local copies, waits for them, and re-layouts  28.6 us (11%)
  between operations  13.7 us (5%)
  other arithmetic  11.4 us (4%)
  starting transfers between devices  9.24 us (4%)
    all_to_all x1, blocking collectives, shards(): lax.all_to_all(outgoing, ('sp', 'tp'), split_axis=0, concat_axis=0, tiled...  63.9 us
    all_to_all x1, waiting for transfers between devices, shards(): lax.all_to_all(served, ('sp', 'tp'), split_axis=0, concat_axis=0, tiled=T...  59.7 us
    all_gather x1, waiting for transfers between devices, whole_out_weight(): return lax.all_gather(own, ('tp', 'sp'), axis=0, tiled=True)  21.5 us
    all_gather x1, blocking collectives, shards(): lax.all_gather(key_rot, 'sp', axis=0, tiled=True)  14.9 us
    dot_general x1, matrix products, shards(): jnp.dot(hidden, w_down[0], preferred_element_type=jnp.float32)  9.66 us
    unnamed x41, local copies, waits for them, and re-layouts  7.63 us
    dot_general x2, matrix products, shards(): jnp.dot(picked[:, choice].astype(jnp.bfloat16), returned, preferred_eleme...  6.52 us
  transfers between devices with their start and end apart: 4, of which 4 were waited for; matrix products, arithmetic and copies ran while one was open for 17% of the time, Pallas kernels for 0%

profile of v1, /device:TPU:0, one launch (start us, length us, event | category | flops | bytes accessed | tf_op | source)
XLA Modules:
  0.0 262.8 jit_solution(14248461183122850936)
XLA Ops:
  7.3 1.9 constant_dynamic-slice_fusion
  9.2 2.0 copy.68
  11.2 3.2 %reshape.201 = bf16[192,4,2,192]{3,2,0,1:T(2,128)(2,1)} reshape(bf16[192,4,384]{2,0,1:T(8,128)(2,1)} %copy.68) | data formatting | bytes 1179648 | tf_op jit(solution)/shard_map/reshape | solution.py:117
  14.4 1.3 slice.43
  16.6 1.9 convert_element_type.90
  18.5 1.8 copy.71
  22.1 1.5 copy.73
  23.6 1.5 copy.72
  25.1 1.3 subtract_convert_fusion
  26.8 14.9 %all_gather.10 = bf16[768,4,64]{2,1,0:T(4,128)(2,1)} all-gather(bf16[192,4,64]{2,1,0:T(4,128)(2,1)S(1)} %pad_maximum_fusion), channel_id=1, replica_groups=mesh['grp'=2,'sp'=4,'tp'=4] {'sp'}, dimensions={0}, use_global_device_ids=true | all-gather | bytes 491520 | tf_op jit(solution)/shard_map/all_gather | solution.py:137
  41.8 2.6 all-gather.3.cloned.1.call-done
  44.4 3.0 %fusion = f32[768,4]{0,1:T(4,128)S(1)} fusion(bf16[768,4,512]{2,1,0:T(4,128)(2,1)} %all-gather.3.cloned.1.call-done), kind=kLoop, calls=%fused_computation.2 | loop fusion | flops 4715520 | bytes 3158016 | tf_op jit(solution)/shard_map/reduce_sum | solution.py:40
  47.4 3.2 %fusion.26 = bf16[768,4,256]{0,2,1:T(8,128)(2,1)S(1)} fusion(f32[512]{0:T(512)S(1)} %copy-done.16, f32[768,4]{0,1:T(4,128)S(1)} %add_rsqrt_fusion, bf16[768,4,512]{2,1,0:T(4,128)(2,1)S(1)} %copy-done.2, bf16[512,256]{1,0:T(8,128)(2,1)} %param.20), kind=kOutput, calls=%fused_computation.31 | convolution fusion | flops 812384256 | bytes 4995072 | tf_op jit(solution)/shard_map/dot_general | solution.py:47
  52.7 1.3 fusion.4
  54.0 2.2 fusion.23
  56.3 1.2 fusion.38
  58.9 4.6 %all-to-all-start = ((bf16[192,4,256]{2,1,0:T(4,128)(2,1)}), bf16[192,4,256]{2,1,0:T(4,128)(2,1)S(1)}, u32[]{:S(2)}, u32[]{:S(2)}) async-start(bf16[192,4,256]{2,1,0:T(4,128)(2,1)} %reshape.214), calls=%async_computation | async-start | bytes 786432 | tf_op jit(solution)/shard_map/all_to_all | solution.py:141
  63.5 2.5 reshape.210
  68.3 1.0 eq.28
  71.4 1.7 iota_compare_fusion
  73.0 3.5 %all-to-all-done = bf16[192,4,256]{2,1,0:T(4,128)(2,1)S(1)} async-done(((bf16[192,4,256]{2,1,0:T(4,128)(2,1)}), bf16[192,4,256]{2,1,0:T(4,128)(2,1)S(1)}, u32[]{:S(2)}, u32[]{:S(2)}) %all-to-all-start) | async-done | bytes 393248 | tf_op jit(solution)/shard_map/all_to_all | solution.py:141
  77.0 21.5 %all-gather.5.cloned.1.call-done = bf16[1024,2048]{1,0:T(8,128)(2,1)} async-done(((bf16[64,2048]{1,0:T(8,128)(2,1)}), bf16[1024,2048]{1,0:T(8,128)(2,1)}) %all-gather.5.cloned.1.call-update) | async-done | bytes 4194320 | tf_op jit(solution)/shard_map/all_gather | solution.py:92
  98.5 3.8 %multiply_reduce_fusion = (f32[192]{0:T(256)S(1)}, f32[192,2048]{1,0:T(8,128)S(1)}) fusion(f32[192,2048]{1,0:T(8,128)} %reshape.210, bf16[192,1024]{1,0:T(8,128)(2,1)S(1)} %bitcast.72, bf16[1024,2048]{1,0:T(8,128)(2,1)} %all-gather.5.cloned.1.call-done), kind=kOutput, calls=%fused_computation.33 | convolution fusion | flops 807272256 | bytes 7734016 | tf_op jit(solution)/shard_map/dot_general | solution.py:144
  103.3 63.9 %all_to_all.25 = bf16[16,40,2048]{2,1,0:T(8,128)(2,1)S(1)} all-to-all(bf16[16,40,2048]{2,1,0:T(8,128)(2,1)S(1)} %bitcast.66), channel_id=1, replica_groups=mesh['grp'=2,'sp'=4,'tp'=4] {'sp','tp'}, dimensions={0} | all-to-all | bytes 5242880 | tf_op jit(solution)/shard_map/all_to_all | solution.py:164
  167.2 1.5 copy-done.4
  168.7 3.5 %fusion.9 = f32[640,768]{1,0:T(8,128)} fusion(bf16[640,2048]{1,0:T(8,128)(2,1)S(1)} %bitcast.70, bf16[1,2048,768]{2,1,0:T(8,128)(2,1)S(1)} %copy-done.14), kind=kOutput, calls=%fused_computation.15 | convolution fusion | flops 2013265920 | bytes 7733248 | tf_op jit(solution)/shard_map/dot_general | solution.py:166
  172.2 9.7 %convolution_convert_fusion = bf16[640,2048]{1,0:T(8,128)(2,1)} fusion(bf16[1,768,2048]{2,1,0:T(8,128)(2,1)S(1)} %copy-done, f32[640,768]{1,0:T(8,128)} %fusion.9, bf16[640,2048]{1,0:T(8,128)(2,1)} %bitcast.71, bf16[1,2048,768]{2,1,0:T(8,128)(2,1)} %param.28), kind=kOutput, calls=%fused_computation.10 | convolution fusion | flops 4030791680 | bytes 13500416 | tf_op jit(solution)/shard_map/dot_general | solution.py:170
  181.9 4.6 %all-to-all-start.2 = ((bf16[16,40,2048]{2,1,0:T(8,128)(2,1)}), bf16[16,40,2048]{2,1,0:T(8,128)(2,1)}, u32[]{:S(2)}, u32[]{:S(2)}) async-start(bf16[16,40,2048]{2,1,0:T(8,128)(2,1)} %bitcast.69), calls=%async_computation.2 | async-start | bytes 5242880 | tf_op jit(solution)/shard_map/all_to_all | solution.py:174
  187.4 59.7 %all-to-all-done.2 = bf16[16,40,2048]{2,1,0:T(8,128)(2,1)} async-done(((bf16[16,40,2048]{2,1,0:T(8,128)(2,1)}), bf16[16,40,2048]{2,1,0:T(8,128)(2,1)}, u32[]{:S(2)}, u32[]{:S(2)}) %all-to-all-start.2) | async-done | bytes 2621472 | tf_op jit(solution)/shard_map/all_to_all | solution.py:174
  247.1 3.0 %fusion.12 = f32[192,2048]{1,0:T(8,128)S(1)} fusion(f32[192,2048]{1,0:T(8,128)} %copy-done.1, bf16[640,2048]{1,0:T(8,128)(2,1)} %bitcast.18, f32[192]{0:T(256)S(1)} %bitcast.75, pred[192,2,640]{2,0,1:T(32,128)(4,1)S(1)} %copy-done.6), kind=kOutput, calls=%fused_computation.21 | convolution fusion | flops 504102912 | bytes 5891072 | tf_op jit(solution)/shard_map/dot_general | solution.py:178
  250.1 3.5 %fusion.13 = bf16[192,2048]{1,0:T(8,128)(2,1)} fusion(f32[192,2048]{1,0:T(8,128)S(1)} %fusion.12, bf16[640,2048]{1,0:T(8,128)(2,1)} %bitcast.18, f32[192]{0:T(256)S(1)} %bitcast.76, pred[192,2,640]{2,0,1:T(32,128)(4,1)S(1)} %copy-done.6), kind=kOutput, calls=%fused_computation.22 | convolution fusion | flops 504496128 | bytes 5104640 | tf_op jit(solution)/shard_map/dot_general | solution.py:178
  253.6 2.4 reshape.209
  (77 shorter events, 14.1 us)
Async XLA Ops:
  6.5 165.7 %copy-start = (bf16[1,768,2048]{2,1,0:T(8,128)(2,1)S(1)}, bf16[1,768,2048]{2,1,0:T(8,128)(2,1)}, u32[]{:S(2)}) copy-start(bf16[1,768,2048]{2,1,0:T(8,128)(2,1)} %param.29) | copy-start | bytes 9437188
  6.5 37.8 %all-gather.3.cloned.1.call-start = ((), (), s32[]{:S(2)}) async-start(), calls=%async_computation.3 | async-start | bytes 3932160 | tf_op jit(solution)/shard_map/all_gather | solution.py:129
  7.3 91.2 %all-gather.5.cloned.1.call-start = ((), (), s32[]{:S(2)}) async-start(), calls=%async_computation.4 | async-start | bytes 4456448 | tf_op jit(solution)/shard_map/all_gather | solution.py:92
  25.1 16.6 %copy-start.5 = (f32[192,4,2,64]{0,3,2,1:T(8,128)S(1)}, f32[192,4,2,64]{0,3,2,1:T(8,128)}, u32[]{:S(2)}) copy-start(f32[192,4,2,64]{0,3,2,1:T(8,128)} %convert_element_type.90) | copy-start | bytes 1179652
  25.1 16.6 %copy-start.8 = (f32[192,32]{0,1:T(8,128)S(1)}, f32[192,32]{0,1:T(8,128)}, u32[]{:S(2)}) copy-start(f32[192,32]{0,1:T(8,128)} %get-tuple-element.13) | copy-start | bytes 73732
  25.1 16.6 %copy-start.9 = (f32[192,32]{0,1:T(8,128)S(1)}, f32[192,32]{0,1:T(8,128)}, u32[]{:S(2)}) copy-start(f32[192,32]{0,1:T(8,128)} %get-tuple-element.14) | copy-start | bytes 73732
  26.8 20.6 %copy-start.16 = (f32[512]{0:T(512)S(1)}, f32[512]{0:T(512)}, u32[]{:S(2)}) copy-start(f32[512]{0:T(512)} %param.19) | copy-start | bytes 6148
  44.4 3.0 %copy-start.2 = (bf16[768,4,512]{2,1,0:T(4,128)(2,1)S(1)}, bf16[768,4,512]{2,1,0:T(4,128)(2,1)}, u32[]{:S(2)}) copy-start(bf16[768,4,512]{2,1,0:T(4,128)(2,1)} %all-gather.3.cloned.1.call-done) | copy-start | bytes 9437188
  47.4 3.2 %slice-start = ((bf16[192,4,2,192]{3,2,0,1:T(2,128)(2,1)}), bf16[192,4,2,128]{3,2,0,1:T(2,128)(2,1)S(1)}, s32[]{:S(2)}) async-start(bf16[192,4,2,192]{3,2,0,1:T(2,128)(2,1)} %reshape.201), calls=%async_computation.5 | async-start | bytes 786432 | tf_op jit(solution)/shard_map/slice | solution.py:118
  50.6 1.1 copy-start.3
  52.7 1.3 copy-start.15
  57.4 8.5 %copy-start.11 = (s32[48,4,2]{0,2,1:T(2,128)S(1)}, s32[48,4,2]{0,2,1:T(2,128)}, u32[]{:S(2)}) copy-start(s32[48,4,2]{0,2,1:T(2,128)} %param.26) | copy-start | bytes 4612
  58.9 17.7 %all-to-all-start = ((bf16[192,4,256]{2,1,0:T(4,128)(2,1)}), bf16[192,4,256]{2,1,0:T(4,128)(2,1)S(1)}, u32[]{:S(2)}, u32[]{:S(2)}) async-start(bf16[192,4,256]{2,1,0:T(4,128)(2,1)} %reshape.214), calls=%async_computation | async-start | bytes 786432 | tf_op jit(solution)/shard_map/all_to_all | solution.py:141
  98.5 3.8 %copy-start.7 = (pred[192,640]{1,0:T(8,128)(4,1)S(1)}, pred[192,640]{1,0:T(8,128)(4,1)}, u32[]{:S(2)}) copy-start(pred[192,640]{1,0:T(8,128)(4,1)} %get-tuple-element.12) | copy-start | bytes 368644
  98.5 3.8 %copy-start.12 = (f32[2048]{0:T(1024)S(1)}, f32[2048]{0:T(1024)}, u32[]{:S(2)}) copy-start(f32[2048]{0:T(1024)} %param.23) | copy-start | bytes 24580
  102.3 64.9 %copy-start.1 = (f32[192,2048]{1,0:T(8,128)}, f32[192,2048]{1,0:T(8,128)S(1)}, u32[]{:S(2)}) copy-start(f32[192,2048]{1,0:T(8,128)S(1)} %get-tuple-element.18) | copy-start | bytes 4718596
  103.3 65.4 %copy-start.14 = (bf16[1,2048,768]{2,1,0:T(8,128)(2,1)S(1)}, bf16[1,2048,768]{2,1,0:T(8,128)(2,1)}, u32[]{:S(2)}) copy-start(bf16[1,2048,768]{2,1,0:T(8,128)(2,1)} %param.27) | copy-start | bytes 9437188
  167.2 1.5 copy-start.4
  181.9 4.6 %copy-start.10 = (f32[48,4,2]{0,2,1:T(2,128)S(1)}, f32[48,4,2]{0,2,1:T(2,128)}, u32[]{:S(2)}) copy-start(f32[48,4,2]{0,2,1:T(2,128)} %param.25) | copy-start | bytes 4612
  181.9 4.8 %copy-start.13 = (f32[48,4]{0,1:T(4,128)S(1)}, f32[48,4]{0,1:T(4,128)}, u32[]{:S(2)}) copy-start(f32[48,4]{0,1:T(4,128)} %param.24) | copy-start | bytes 2308
  181.9 65.2 %copy-start.6 = (pred[192,2,640]{2,0,1:T(32,128)(4,1)S(1)}, pred[192,2,640]{2,0,1:T(32,128)(4,1)}, u32[]{:S(2)}) copy-start(pred[192,2,640]{2,0,1:T(32,128)(4,1)} %get-tuple-element.11) | copy-start | bytes 737284
  181.9 65.2 %all-to-all-start.2 = ((bf16[16,40,2048]{2,1,0:T(8,128)(2,1)}), bf16[16,40,2048]{2,1,0:T(8,128)(2,1)}, u32[]{:S(2)}, u32[]{:S(2)}) async-start(bf16[16,40,2048]{2,1,0:T(8,128)(2,1)} %bitcast.69), calls=%async_computation.2 | async-start | bytes 5242880 | tf_op jit(solution)/shard_map/all_to_all | solution.py:174
Sparse Core Ops, SparseCore 0:
  8.9 35.4 all-gather.2
  46.5 51.8 all-gather.4

commit v2 on v1

--- a/solution.py
+++ b/solution.py
@@ -1,6 +1,8 @@
 import jax
 import jax.numpy as jnp
 from jax import lax
+from jax.experimental import pallas as pl
+from jax.experimental.pallas import tpu as pltpu
 from jax.sharding import PartitionSpec as P
 
 D = 2048
@@ -86,10 +88,102 @@
 
 
 def whole_out_weight(out_weight):
-    pieces = lax.axis_size("sp")
-    depth = out_weight.shape[0] // pieces
-    own = lax.dynamic_slice_in_dim(out_weight, lax.axis_index("sp") * depth, depth, axis=0)
-    return lax.all_gather(own, ("tp", "sp"), axis=0, tiled=True)
+    copies = ("grp", "sp")
+    depth = out_weight.shape[0] // lax.axis_size(copies)
+    own = lax.dynamic_slice_in_dim(out_weight, lax.axis_index(copies) * depth, depth, axis=0)
+    return lax.all_gather(own, ("tp",) + copies, axis=0, tiled=True)
+
+
+def gather_kernel(chips, pieces, latent_ref, rot_ref, latent_out, rot_out, *sems):
+    near_send, near_recv, far_send, far_recv, own_sem = sems
+    me = lax.axis_index("sp")
+    chip, core = me // 2, lax.rem(me, 2)
+    mate = chip * 2 + 1 - core
+    mesh_id = pl.DeviceIdType.MESH
+
+    def peer(step):
+        return lax.rem(chip + step, chips) * 2 + core
+
+    barrier = pltpu.get_barrier_semaphore()
+    pl.semaphore_signal(barrier, inc=1, device_id={"sp": mate}, device_id_type=mesh_id)
+    for step in range(1, chips):
+        pl.semaphore_signal(barrier, inc=1, device_id={"sp": peer(step)}, device_id_type=mesh_id)
+    pl.semaphore_wait(barrier, chips)
+
+    rows = latent_ref.shape[0] // pieces
+
+    def views(slot, piece, own):
+        if piece == pieces:
+            return (rot_ref if own else rot_out.at[slot]), rot_out.at[slot]
+        part = pl.ds(piece * rows, rows)
+        target = latent_out.at[slot, part]
+        return (latent_ref.at[part] if own else target), target
+
+    def remote(slot, piece, own, send, recv, device):
+        source, target = views(slot, piece, own)
+        copy = pltpu.make_async_remote_copy(
+            src_ref=source,
+            dst_ref=target,
+            send_sem=send,
+            recv_sem=recv,
+            device_id={"sp": device},
+            device_id_type=mesh_id,
+        )
+        copy.start()
+        return copy
+
+    order = [pieces] + list(range(pieces))
+    far = {}
+    for step in range(1, chips):
+        for piece in order:
+            far[step, piece] = remote(
+                me, piece, True, far_send.at[step, piece], far_recv.at[step, piece], peer(step)
+            )
+    near = []
+    for piece in order:
+        near.append(
+            remote(me, piece, True, near_send.at[0, piece], near_recv.at[0, piece], mate)
+        )
+    kept = [
+        pltpu.make_async_copy(latent_ref, latent_out.at[me], own_sem.at[0]),
+        pltpu.make_async_copy(rot_ref, rot_out.at[me], own_sem.at[1]),
+    ]
+    for copy in kept:
+        copy.start()
+    for step in range(1, chips):
+        slot = peer(chips - step)
+        for piece in order:
+            far[step, piece].wait_recv()
+            near.append(
+                remote(
+                    slot, piece, False, near_send.at[step, piece], near_recv.at[step, piece], mate
+                )
+            )
+    for copy in kept:
+        copy.wait()
+    for copy in far.values():
+        copy.wait_send()
+    for copy in near:
+        copy.wait()
+
+
+def gather_keys(latent, key_rot):
+    count = lax.axis_size("sp")
+    chips, pieces = count // 2, 6
+    outs = pl.pallas_call(
+        lambda *refs: gather_kernel(chips, pieces, *refs),
+        out_shape=[
+            jax.ShapeDtypeStruct((count,) + latent.shape, latent.dtype),
+            jax.ShapeDtypeStruct((count,) + key_rot.shape, key_rot.dtype),
+        ],
+        in_specs=[pl.BlockSpec(memory_space=pl.ANY)] * 2,
+        out_specs=[pl.BlockSpec(memory_space=pl.ANY)] * 2,
+        scratch_shapes=[pltpu.SemaphoreType.DMA((chips, pieces + 1))] * 4
+        + [pltpu.SemaphoreType.DMA((2,))],
+        compiler_params=pltpu.CompilerParams(collective_id=0, has_side_effects=True),
+        name="gather_keys",
+    )(latent, key_rot)
+    return [whole.reshape((-1,) + whole.shape[2:]) for whole in outs]
 
 
 def shards(
@@ -125,16 +219,15 @@
         jnp.zeros((positions_here, SEQS, heads_here), jnp.float32),
         jnp.zeros((positions_here, SEQS, heads_here, VDIM), jnp.float32),
     )
-    key_nope, value_rows = expand(
-        lax.all_gather(latent, "sp", axis=0, tiled=True), latent_gain, key_up, value_up
-    )
+    all_latent, all_key_rot = gather_keys(latent, key_rot)
+    key_nope, value_rows = expand(all_latent, latent_gain, key_up, value_up)
     finished = absorb(
         initial,
         query_nope,
         query_rot,
         key_nope,
         value_rows,
-        lax.all_gather(key_rot, "sp", axis=0, tiled=True),
+        all_key_rot,
     )
     attended = (finished[2] / finished[1][..., None]).astype(jnp.bfloat16)
     attended = attended.reshape(positions_here, SEQS, heads_here * VDIM)

time: 264 us -> 262 us (level)
  Pallas kernels: 0 us -> 34.5 us
  waiting for transfers between devices: 88 us -> 60.8 us
  blocking collectives: 78.8 us -> 64.5 us
  other arithmetic: 11.4 us -> 16.9 us
    pallas_call x0 -> x1, Pallas kernels: none -> 34.5 us  [gather_keys(): pl.pallas_call(lambda *refs: gather_kernel(chips, pieces, *refs), out_sha...]
    all_gather x2 -> x1, waiting for transfers between devices: 24.1 us -> 0.02 us  [whole_out_weight(): return lax.all_gather(own, ('tp',) + copies, axis=0, tiled=True)]
    all_gather x1 -> x0, blocking collectives: 14.9 us -> none  [shards(): lax.all_gather(key_rot, 'sp', axis=0, tiled=True)]
    convert_element_type x0 -> x1, other arithmetic: none -> 2.86 us  [expand(): latent_rows.astype(jnp.float32)]
    unnamed x41 -> x37, local copies, waits for them, and re-layouts: 7.63 us -> 6.76 us
  transfers between devices with their start and end apart: 4 -> 3, of which waited for: 4 -> 2; matrix products, arithmetic and copies ran while one was open for 17% -> 18% of each run, Pallas kernels for 0% -> 13%
where the time goes in v2:
time: 262 us
  blocking collectives  64.5 us (25%)
  waiting for transfers between devices  60.8 us (23%)
  Pallas kernels  34.5 us (13%)
  matrix products  33.9 us (13%)
  local copies, waits for them, and re-layouts  27.4 us (10%)
  other arithmetic  16.9 us (6%)
  between operations  13.7 us (5%)
  starting transfers between devices  9.75 us (4%)
    all_to_all x1, blocking collectives, shards(): lax.all_to_all(outgoing, ('sp', 'tp'), split_axis=0, concat_axis=0, tiled...  64.5 us
    all_to_all x1, waiting for transfers between devices, shards(): lax.all_to_all(served, ('sp', 'tp'), split_axis=0, concat_axis=0, tiled=T...  59.5 us
    pallas_call x1, Pallas kernels, gather_keys(): pl.pallas_call(lambda *refs: gather_kernel(chips, pieces, *refs), out_sha...  34.5 us
    dot_general x1, matrix products, shards(): jnp.dot(hidden, w_down[0], preferred_element_type=jnp.float32)  9.64 us
    unnamed x37, local copies, waits for them, and re-layouts  6.76 us
    dot_general x2, matrix products, shards(): jnp.dot(picked[:, choice].astype(jnp.bfloat16), returned, preferred_eleme...  6.52 us
  transfers between devices with their start and end apart: 3, of which 2 were waited for; matrix products, arithmetic and copies ran while one was open for 18% of the time, Pallas kernels for 13%

profile of v2, /device:TPU:0, one launch (start us, length us, event | category | flops | bytes accessed | tf_op | source)
XLA Modules:
  0.0 261.6 jit_solution(13018107937672552425)
XLA Ops:
  6.5 1.7 constant_dynamic-slice_fusion
  8.3 2.0 copy.74
  10.3 3.2 %reshape.216 = bf16[192,4,2,192]{3,2,0,1:T(2,128)(2,1)} reshape(bf16[192,4,384]{2,0,1:T(8,128)(2,1)} %copy.74) | data formatting | bytes 1179648 | tf_op jit(solution)/shard_map/reshape | solution.py:211
  16.2 1.5 copy.69
  17.6 1.5 copy.68
  19.2 1.3 subtract_convert_fusion
  21.4 34.5 %gather_keys.1 = (bf16[4,192,4,512]{3,2,1,0:T(4,128)(2,1)}, bf16[4,192,4,64]{3,2,1,0:T(4,128)(2,1)}) custom-call(bf16[192,4,512]{2,1,0:T(4,128)(2,1)} %refs_0_.1, bf16[192,4,64]{2,1,0:T(4,128)(2,1)} %pad_maximum_fusion.refs_1_), custom_call_target="tpu_custom_call" | custom-call | tf_op jit(solution)/shard_map/gather_keys/pallas_call | solution.py:173
  55.9 4.2 %multiply_reduce_fusion = f32[4,192,4]{2,1,0:T(8,128)S(1)} fusion(bf16[4,192,4,512]{3,2,1,0:T(4,128)(2,1)} %get-tuple-element.7), kind=kLoop, calls=%fused_computation.3 | loop fusion | flops 4715520 | bytes 3158016 | tf_op jit(solution)/shard_map/reduce_sum | solution.py:42
  60.9 1.1 copy.70
  62.1 1.0 copy.102
  64.9 2.9 %bitcast_convert_fusion = f32[768,4,512]{2,1,0:T(4,128)S(1)} fusion(bf16[4,192,4,512]{3,2,1,0:T(4,128)(2,1)} %get-tuple-element.7), kind=kLoop, calls=%fused_computation.74 | loop fusion | flops 1572864 | bytes 9437184 | tf_op jit(solution)/shard_map/convert_element_type | solution.py:48
  67.8 3.0 %convolution_convert_fusion.2 = bf16[768,4,256]{0,2,1:T(8,128)(2,1)S(1)} fusion(f32[768,4,512]{2,1,0:T(4,128)S(1)} %bitcast_convert_fusion, f32[512]{0:T(512)S(1)} %copy-done.10, f32[768,4]{0,1:T(4,128)S(1)} %copy.70, bf16[512,256]{1,0:T(8,128)(2,1)S(1)} %copy-done.6), kind=kOutput, calls=%fused_computation.27 | convolution fusion | flops 810811392 | bytes 8140800 | tf_op jit(solution)/shard_map/dot_general | solution.py:49
  72.0 1.1 fusion.50
  73.1 1.4 fusion.3
  74.5 3.0 %convolution_convert_fusion.3 = bf16[768,4,256]{0,2,1:T(8,128)(2,1)S(1)} fusion(f32[768,4,512]{2,1,0:T(4,128)S(1)} %bitcast_convert_fusion, f32[512]{0:T(512)S(1)} %copy-done.10, f32[768,4]{0,1:T(4,128)S(1)} %copy.70, bf16[512,256]{1,0:T(8,128)(2,1)S(1)} %copy-done.7), kind=kOutput, calls=%fused_computation.28 | convolution fusion | flops 810811392 | bytes 8140800 | tf_op jit(solution)/shard_map/dot_general | solution.py:50
  77.5 1.4 fusion.27
  79.3 1.0 reshape.231
  80.3 4.9 %all-to-all-start = ((bf16[192,4,256]{2,1,0:T(4,128)(2,1)}), bf16[192,4,256]{2,1,0:T(4,128)(2,1)S(1)}, u32[]{:S(2)}, u32[]{:S(2)}) async-start(bf16[192,4,256]{2,1,0:T(4,128)(2,1)} %reshape.231), calls=%async_computation | async-start | bytes 786432 | tf_op jit(solution)/shard_map/all_to_all | solution.py:234
  85.3 2.5 reshape.226
  90.1 1.0 eq.28
  93.2 1.7 iota_compare_fusion
  94.8 1.3 all-to-all-done
  96.6 3.8 %multiply_reduce_fusion.1 = (f32[192]{0:T(256)S(1)}, f32[192,2048]{1,0:T(8,128)S(1)}) fusion(f32[192,2048]{1,0:T(8,128)} %reshape.226, bf16[192,1024]{1,0:T(8,128)(2,1)S(1)} %bitcast.78, bf16[1024,2048]{1,0:T(8,128)(2,1)} %all-gather.2.cloned.1.call-done), kind=kOutput, calls=%fused_computation.30 | convolution fusion | flops 807272256 | bytes 7734016 | tf_op jit(solution)/shard_map/dot_general | solution.py:237
  101.4 64.5 %all_to_all.25 = bf16[16,40,2048]{2,1,0:T(8,128)(2,1)S(1)} all-to-all(bf16[16,40,2048]{2,1,0:T(8,128)(2,1)S(1)} %bitcast.73), channel_id=1, replica_groups=mesh['grp'=2,'sp'=4,'tp'=4] {'sp','tp'}, dimensions={0} | all-to-all | bytes 5242880 | tf_op jit(solution)/shard_map/all_to_all | solution.py:257
  166.0 1.5 copy-done.2
  167.5 3.5 %fusion.8 = f32[640,768]{1,0:T(8,128)} fusion(bf16[640,2048]{1,0:T(8,128)(2,1)S(1)} %bitcast.76, bf16[1,2048,768]{2,1,0:T(8,128)(2,1)S(1)} %copy-done.14), kind=kOutput, calls=%fused_computation.14 | convolution fusion | flops 2013265920 | bytes 7733248 | tf_op jit(solution)/shard_map/dot_general | solution.py:259
  171.0 9.6 %convolution_convert_fusion = bf16[640,2048]{1,0:T(8,128)(2,1)} fusion(bf16[1,768,2048]{2,1,0:T(8,128)(2,1)S(1)} %copy-done, f32[640,768]{1,0:T(8,128)} %fusion.8, bf16[640,2048]{1,0:T(8,128)(2,1)} %bitcast.77, bf16[1,2048,768]{2,1,0:T(8,128)(2,1)} %param.28), kind=kOutput, calls=%fused_computation.9 | convolution fusion | flops 4030791680 | bytes 13500416 | tf_op jit(solution)/shard_map/dot_general | solution.py:263
  180.7 4.8 %all-to-all-start.2 = ((bf16[16,40,2048]{2,1,0:T(8,128)(2,1)}), bf16[16,40,2048]{2,1,0:T(8,128)(2,1)}, u32[]{:S(2)}, u32[]{:S(2)}) async-start(bf16[16,40,2048]{2,1,0:T(8,128)(2,1)} %bitcast.75), calls=%async_computation.2 | async-start | bytes 5242880 | tf_op jit(solution)/shard_map/all_to_all | solution.py:267
  186.4 59.5 %all-to-all-done.2 = bf16[16,40,2048]{2,1,0:T(8,128)(2,1)} async-done(((bf16[16,40,2048]{2,1,0:T(8,128)(2,1)}), bf16[16,40,2048]{2,1,0:T(8,128)(2,1)}, u32[]{:S(2)}, u32[]{:S(2)}) %all-to-all-start.2) | async-done | bytes 2621472 | tf_op jit(solution)/shard_map/all_to_all | solution.py:267
  245.8 3.0 %fusion.11 = f32[192,2048]{1,0:T(8,128)S(1)} fusion(f32[192,2048]{1,0:T(8,128)} %copy-done.1, bf16[640,2048]{1,0:T(8,128)(2,1)} %bitcast.21, f32[192]{0:T(256)S(1)} %bitcast.83, pred[192,2,640]{2,0,1:T(32,128)(4,1)S(1)} %copy-done.3), kind=kOutput, calls=%fused_computation.20 | convolution fusion | flops 504102912 | bytes 5891072 | tf_op jit(solution)/shard_map/dot_general | solution.py:271
  248.9 3.5 %fusion.12 = bf16[192,2048]{1,0:T(8,128)(2,1)} fusion(f32[192,2048]{1,0:T(8,128)S(1)} %fusion.11, bf16[640,2048]{1,0:T(8,128)(2,1)} %bitcast.21, f32[192]{0:T(256)S(1)} %bitcast.84, pred[192,2,640]{2,0,1:T(32,128)(4,1)S(1)} %copy-done.3), kind=kOutput, calls=%fused_computation.21 | convolution fusion | flops 504496128 | bytes 5104640 | tf_op jit(solution)/shard_map/dot_general | solution.py:271
  252.4 2.4 reshape.225
  (73 shorter events, 14.5 us)
Async XLA Ops:
  6.5 164.5 %copy-start = (bf16[1,768,2048]{2,1,0:T(8,128)(2,1)S(1)}, bf16[1,768,2048]{2,1,0:T(8,128)(2,1)}, u32[]{:S(2)}) copy-start(bf16[1,768,2048]{2,1,0:T(8,128)(2,1)} %param.29) | copy-start | bytes 9437188
  6.5 7.0 %copy-start.8 = (bf16[192,4,64]{0,2,1:T(8,128)(2,1)S(1)}, bf16[192,4,64]{0,2,1:T(8,128)(2,1)}, u32[]{:S(2)}) copy-start(bf16[192,4,64]{0,2,1:T(8,128)(2,1)} %param.18) | copy-start | bytes 294916
  6.5 90.0 %all-gather.2.cloned.1.call-start = ((), (), s32[]{:S(2)}) async-start(), calls=%async_computation.3 | async-start | bytes 4325376 | tf_op jit(solution)/shard_map/all_gather | solution.py:94
  21.4 40.6 %slice-start = ((bf16[192,4,2,192]{3,2,0,1:T(2,128)(2,1)}), bf16[192,4,2,64]{3,2,0,1:T(2,128)(2,1)S(1)}, s32[]{:S(2)}) async-start(bf16[192,4,2,192]{3,2,0,1:T(2,128)(2,1)} %reshape.216), calls=%async_computation.4 | async-start | bytes 786432 | tf_op jit(solution)/shard_map/slice | solution.py:213
  64.9 2.9 %copy-start.6 = (bf16[512,256]{1,0:T(8,128)(2,1)S(1)}, bf16[512,256]{1,0:T(8,128)(2,1)}, u32[]{:S(2)}) copy-start(bf16[512,256]{1,0:T(8,128)(2,1)} %param.20) | copy-start | bytes 786436
  64.9 2.9 %copy-start.10 = (f32[512]{0:T(512)S(1)}, f32[512]{0:T(512)}, u32[]{:S(2)}) copy-start(f32[512]{0:T(512)} %param.19) | copy-start | bytes 6148
  67.8 3.1 %slice-start.1 = ((bf16[192,4,2,192]{3,2,0,1:T(2,128)(2,1)}), bf16[192,4,2,128]{3,2,0,1:T(2,128)(2,1)S(1)}, s32[]{:S(2)}) async-start(bf16[192,4,2,192]{3,2,0,1:T(2,128)(2,1)} %reshape.216), calls=%async_computation.5 | async-start | bytes 786432 | tf_op jit(solution)/shard_map/slice | solution.py:212
  70.9 1.1 copy-start.4
  73.1 1.4 copy-start.7
  78.9 8.8 %copy-start.11 = (s32[48,4,2]{0,2,1:T(2,128)S(1)}, s32[48,4,2]{0,2,1:T(2,128)}, u32[]{:S(2)}) copy-start(s32[48,4,2]{0,2,1:T(2,128)} %param.26) | copy-start | bytes 4612
  80.3 15.9 %all-to-all-start = ((bf16[192,4,256]{2,1,0:T(4,128)(2,1)}), bf16[192,4,256]{2,1,0:T(4,128)(2,1)S(1)}, u32[]{:S(2)}, u32[]{:S(2)}) async-start(bf16[192,4,256]{2,1,0:T(4,128)(2,1)} %reshape.231), calls=%async_computation | async-start | bytes 786432 | tf_op jit(solution)/shard_map/all_to_all | solution.py:234
  96.6 3.9 %copy-start.5 = (pred[192,640]{1,0:T(8,128)(4,1)S(1)}, pred[192,640]{1,0:T(8,128)(4,1)}, u32[]{:S(2)}) copy-start(pred[192,640]{1,0:T(8,128)(4,1)} %get-tuple-element.16) | copy-start | bytes 368644
  96.6 3.9 %copy-start.12 = (f32[2048]{0:T(1024)S(1)}, f32[2048]{0:T(1024)}, u32[]{:S(2)}) copy-start(f32[2048]{0:T(1024)} %param.23) | copy-start | bytes 24580
  100.4 65.5 %copy-start.1 = (f32[192,2048]{1,0:T(8,128)}, f32[192,2048]{1,0:T(8,128)S(1)}, u32[]{:S(2)}) copy-start(f32[192,2048]{1,0:T(8,128)S(1)} %get-tuple-element.22) | copy-start | bytes 4718596
  101.4 66.1 %copy-start.14 = (bf16[1,2048,768]{2,1,0:T(8,128)(2,1)S(1)}, bf16[1,2048,768]{2,1,0:T(8,128)(2,1)}, u32[]{:S(2)}) copy-start(bf16[1,2048,768]{2,1,0:T(8,128)(2,1)} %param.27) | copy-start | bytes 9437188
  165.9 1.5 copy-start.2
  180.6 4.8 %copy-start.9 = (f32[48,4,2]{0,2,1:T(2,128)S(1)}, f32[48,4,2]{0,2,1:T(2,128)}, u32[]{:S(2)}) copy-start(f32[48,4,2]{0,2,1:T(2,128)} %param.25) | copy-start | bytes 4612
  180.6 5.0 %copy-start.13 = (f32[48,4]{0,1:T(4,128)S(1)}, f32[48,4]{0,1:T(4,128)}, u32[]{:S(2)}) copy-start(f32[48,4]{0,1:T(4,128)} %param.24) | copy-start | bytes 2308
  180.7 65.2 %copy-start.3 = (pred[192,2,640]{2,0,1:T(32,128)(4,1)S(1)}, pred[192,2,640]{2,0,1:T(32,128)(4,1)}, u32[]{:S(2)}) copy-start(pred[192,2,640]{2,0,1:T(32,128)(4,1)} %get-tuple-element.15) | copy-start | bytes 737284
  180.7 65.2 %all-to-all-start.2 = ((bf16[16,40,2048]{2,1,0:T(8,128)(2,1)}), bf16[16,40,2048]{2,1,0:T(8,128)(2,1)}, u32[]{:S(2)}, u32[]{:S(2)}) async-start(bf16[16,40,2048]{2,1,0:T(8,128)(2,1)} %bitcast.75), calls=%async_computation.2 | async-start | bytes 5242880 | tf_op jit(solution)/shard_map/all_to_all | solution.py:267
Sparse Core Ops, SparseCore 0:
  10.2 65.0 all-gather.1

commit v3 on v2

--- a/solution.py
+++ b/solution.py
@@ -87,11 +87,12 @@
     return capacity, chosen * capacity + slot_index
 
 
-def whole_out_weight(out_weight):
+def whole_out_weight(out_weight, after):
     copies = ("grp", "sp")
     depth = out_weight.shape[0] // lax.axis_size(copies)
     own = lax.dynamic_slice_in_dim(out_weight, lax.axis_index(copies) * depth, depth, axis=0)
-    return lax.all_gather(own, ("tp",) + copies, axis=0, tiled=True)
+    own, after = lax.optimization_barrier((own, after))
+    return after, lax.all_gather(own, ("tp",) + copies, axis=0, tiled=True)
 
 
 def gather_kernel(chips, pieces, latent_ref, rot_ref, latent_out, rot_out, *sems):
@@ -220,6 +221,7 @@
         jnp.zeros((positions_here, SEQS, heads_here, VDIM), jnp.float32),
     )
     all_latent, all_key_rot = gather_keys(latent, key_rot)
+    all_key_rot, gathered_weight = whole_out_weight(out_weight, all_key_rot)
     key_nope, value_rows = expand(all_latent, latent_gain, key_up, value_up)
     finished = absorb(
         initial,
@@ -236,7 +238,7 @@
     mixed_heads = by_token.reshape(row_count, by_token.shape[2])
     projected = jnp.dot(
         mixed_heads,
-        whole_out_weight(out_weight),
+        gathered_weight,
         preferred_element_type=jnp.float32,
     )
     stream = (residual.reshape(row_count, D).astype(jnp.float32) + projected).astype(jnp.bfloat16)

time: 262 us -> 281 us (1.073)
  waiting for transfers between devices: 60.8 us -> 78.5 us
    all_gather x1, waiting for transfers between devices: 0.02 us -> 16.1 us  [whole_out_weight(): return (after, lax.all_gather(own, ('tp',) + copies, axis=0, tiled=True))]
    unnamed x37 -> x35, local copies, waits for them, and re-layouts: 6.76 us -> 7.82 us
  transfers between devices with their start and end apart: 3 -> 3, of which waited for: 2 -> 3; matrix products, arithmetic and copies ran while one was open for 18% -> 14% of each run, Pallas kernels for 13% -> 0%
where the time goes in v3:
time: 281 us; the launch traced here: 280 us
  waiting for transfers between devices  78.5 us (28%)
  blocking collectives  65.1 us (23%)
  Pallas kernels  34.5 us (12%)
  matrix products  33.8 us (12%)
  local copies, waits for them, and re-layouts  28.4 us (10%)
  other arithmetic  16.4 us (6%)
  between operations  13.7 us (5%)
  starting transfers between devices  9.43 us (3%)
    all_to_all x1, blocking collectives, shards(): lax.all_to_all(outgoing, ('sp', 'tp'), split_axis=0, concat_axis=0, tiled...  65.1 us
    all_to_all x1, waiting for transfers between devices, shards(): lax.all_to_all(served, ('sp', 'tp'), split_axis=0, concat_axis=0, tiled=T...  59.7 us
    pallas_call x1, Pallas kernels, gather_keys(): pl.pallas_call(lambda *refs: gather_kernel(chips, pieces, *refs), out_sha...  34.5 us
    all_gather x1, waiting for transfers between devices, whole_out_weight(): return (after, lax.all_gather(own, ('tp',) + copies, axis=0, tiled=True))  16.1 us
    dot_general x1, matrix products, shards(): jnp.dot(hidden, w_down[0], preferred_element_type=jnp.float32)  9.63 us
    unnamed x35, local copies, waits for them, and re-layouts  7.82 us
    dot_general x2, matrix products, shards(): jnp.dot(picked[:, choice].astype(jnp.bfloat16), returned, preferred_eleme...  6.53 us
  transfers between devices with their start and end apart: 3, of which 3 were waited for; matrix products, arithmetic and copies ran while one was open for 14% of the time, Pallas kernels for 0%

profile of v3, /device:TPU:0, one launch (start us, length us, event | category | flops | bytes accessed | tf_op | source)
XLA Modules:
  0.0 279.7 jit_solution(11454025418585199271)
XLA Ops:
  6.6 1.9 copy.67
  10.3 1.5 copy.69
  11.8 1.5 copy.68
  13.3 1.3 subtract_convert_fusion
  15.5 34.5 %gather_keys.1 = (bf16[4,192,4,512]{3,2,1,0:T(4,128)(2,1)}, bf16[4,192,4,64]{3,2,1,0:T(4,128)(2,1)}) custom-call(bf16[192,4,512]{2,1,0:T(4,128)(2,1)} %refs_0_.1, bf16[192,4,64]{2,1,0:T(4,128)(2,1)} %pad_maximum_fusion.refs_1_), custom_call_target="tpu_custom_call" | custom-call | tf_op jit(solution)/shard_map/gather_keys/pallas_call | solution.py:174
  50.0 1.6 constant_dynamic-slice_fusion
  51.6 2.0 copy.74
  53.6 3.2 %reshape.216 = bf16[192,4,2,192]{3,2,0,1:T(2,128)(2,1)} reshape(bf16[192,4,384]{2,0,1:T(8,128)(2,1)} %copy.74) | data formatting | bytes 1179648 | tf_op jit(solution)/shard_map/reshape | solution.py:212
  56.8 3.6 %multiply_reduce_fusion = f32[4,192,4]{2,1,0:T(8,128)S(1)} fusion(bf16[4,192,4,512]{3,2,1,0:T(4,128)(2,1)} %get-tuple-element.9), kind=kLoop, calls=%fused_computation.3 | loop fusion | flops 4715520 | bytes 3158016 | tf_op jit(solution)/shard_map/reduce_sum | solution.py:42
  61.3 1.1 copy.70
  65.3 2.8 %bitcast_convert_fusion = f32[768,4,512]{2,1,0:T(4,128)S(1)} fusion(bf16[4,192,4,512]{3,2,1,0:T(4,128)(2,1)} %get-tuple-element.9), kind=kLoop, calls=%fused_computation.74 | loop fusion | flops 1572864 | bytes 9437184 | tf_op jit(solution)/shard_map/convert_element_type | solution.py:48
  68.2 3.0 %convolution_convert_fusion.2 = bf16[768,4,256]{0,2,1:T(8,128)(2,1)S(1)} fusion(f32[768,4,512]{2,1,0:T(4,128)S(1)} %bitcast_convert_fusion, f32[512]{0:T(512)S(1)} %copy-done.9, f32[768,4]{0,1:T(4,128)S(1)} %copy.70, bf16[512,256]{1,0:T(8,128)(2,1)S(1)} %copy-done.6), kind=kOutput, calls=%fused_computation.27 | convolution fusion | flops 810811392 | bytes 8140800 | tf_op jit(solution)/shard_map/dot_general | solution.py:49
  72.4 1.1 fusion.50
  73.5 1.4 fusion.3
  74.9 3.0 %convolution_convert_fusion.3 = bf16[768,4,256]{0,2,1:T(8,128)(2,1)S(1)} fusion(f32[768,4,512]{2,1,0:T(4,128)S(1)} %bitcast_convert_fusion, f32[512]{0:T(512)S(1)} %copy-done.9, f32[768,4]{0,1:T(4,128)S(1)} %copy.70, bf16[512,256]{1,0:T(8,128)(2,1)S(1)} %copy-done.7), kind=kOutput, calls=%fused_computation.28 | convolution fusion | flops 810811392 | bytes 8140800 | tf_op jit(solution)/shard_map/dot_general | solution.py:50
  77.9 1.2 fusion.27
  80.5 4.9 %all-to-all-start = ((bf16[192,4,256]{2,1,0:T(4,128)(2,1)}), bf16[192,4,256]{2,1,0:T(4,128)(2,1)S(1)}, u32[]{:S(2)}, u32[]{:S(2)}) async-start(bf16[192,4,256]{2,1,0:T(4,128)(2,1)} %reshape.231), calls=%async_computation | async-start | bytes 786432 | tf_op jit(solution)/shard_map/all_to_all | solution.py:236
  85.4 2.5 reshape.226
  90.3 1.0 eq.28
  93.3 1.7 iota_compare_fusion
  94.9 2.8 all-to-all-done
  98.1 16.1 %all-gather.2.cloned.1.call-done = bf16[1024,2048]{1,0:T(8,128)(2,1)} async-done(((bf16[32,2048]{1,0:T(8,128)(2,1)}), bf16[1024,2048]{1,0:T(8,128)(2,1)}) %all-gather.2.cloned.1.call-update) | async-done | bytes 4194320 | tf_op jit(solution)/shard_map/all_gather | solution.py:95
  114.2 3.8 %multiply_reduce_fusion.1 = (f32[192]{0:T(256)S(1)}, f32[192,2048]{1,0:T(8,128)S(1)}) fusion(f32[192,2048]{1,0:T(8,128)} %reshape.226, bf16[192,1024]{1,0:T(8,128)(2,1)S(1)} %bitcast.77, bf16[1024,2048]{1,0:T(8,128)(2,1)} %all-gather.2.cloned.1.call-done), kind=kOutput, calls=%fused_computation.30 | convolution fusion | flops 807272256 | bytes 7734016 | tf_op jit(solution)/shard_map/dot_general | solution.py:239
  119.0 65.1 %all_to_all.25 = bf16[16,40,2048]{2,1,0:T(8,128)(2,1)S(1)} all-to-all(bf16[16,40,2048]{2,1,0:T(8,128)(2,1)S(1)} %bitcast.72), channel_id=1, replica_groups=mesh['grp'=2,'sp'=4,'tp'=4] {'sp','tp'}, dimensions={0} | all-to-all | bytes 5242880 | tf_op jit(solution)/shard_map/all_to_all | solution.py:259
  184.1 1.5 copy-done.2
  185.6 3.5 %fusion.8 = f32[640,768]{1,0:T(8,128)} fusion(bf16[640,2048]{1,0:T(8,128)(2,1)S(1)} %bitcast.75, bf16[1,2048,768]{2,1,0:T(8,128)(2,1)S(1)} %copy-done.13), kind=kOutput, calls=%fused_computation.14 | convolution fusion | flops 2013265920 | bytes 7733248 | tf_op jit(solution)/shard_map/dot_general | solution.py:261
  189.1 9.6 %convolution_convert_fusion = bf16[640,2048]{1,0:T(8,128)(2,1)} fusion(bf16[1,768,2048]{2,1,0:T(8,128)(2,1)S(1)} %copy-done, f32[640,768]{1,0:T(8,128)} %fusion.8, bf16[640,2048]{1,0:T(8,128)(2,1)} %bitcast.76, bf16[1,2048,768]{2,1,0:T(8,128)(2,1)} %param.28), kind=kOutput, calls=%fused_computation.9 | convolution fusion | flops 4030791680 | bytes 13500416 | tf_op jit(solution)/shard_map/dot_general | solution.py:265
  198.7 4.6 %all-to-all-start.2 = ((bf16[16,40,2048]{2,1,0:T(8,128)(2,1)}), bf16[16,40,2048]{2,1,0:T(8,128)(2,1)}, u32[]{:S(2)}, u32[]{:S(2)}) async-start(bf16[16,40,2048]{2,1,0:T(8,128)(2,1)} %bitcast.74), calls=%async_computation.2 | async-start | bytes 5242880 | tf_op jit(solution)/shard_map/all_to_all | solution.py:269
  204.2 59.7 %all-to-all-done.2 = bf16[16,40,2048]{2,1,0:T(8,128)(2,1)} async-done(((bf16[16,40,2048]{2,1,0:T(8,128)(2,1)}), bf16[16,40,2048]{2,1,0:T(8,128)(2,1)}, u32[]{:S(2)}, u32[]{:S(2)}) %all-to-all-start.2) | async-done | bytes 2621472 | tf_op jit(solution)/shard_map/all_to_all | solution.py:269
  263.9 3.0 %fusion.11 = f32[192,2048]{1,0:T(8,128)S(1)} fusion(f32[192,2048]{1,0:T(8,128)} %copy-done.1, bf16[640,2048]{1,0:T(8,128)(2,1)} %bitcast.21, f32[192]{0:T(256)S(1)} %bitcast.82, pred[192,2,640]{2,0,1:T(32,128)(4,1)S(1)} %copy-done.3), kind=kOutput, calls=%fused_computation.20 | convolution fusion | flops 504102912 | bytes 5891072 | tf_op jit(solution)/shard_map/dot_general | solution.py:273
  266.9 3.5 %fusion.12 = bf16[192,2048]{1,0:T(8,128)(2,1)} fusion(f32[192,2048]{1,0:T(8,128)S(1)} %fusion.11, bf16[640,2048]{1,0:T(8,128)(2,1)} %bitcast.21, f32[192]{0:T(256)S(1)} %bitcast.83, pred[192,2,640]{2,0,1:T(32,128)(4,1)S(1)} %copy-done.3), kind=kOutput, calls=%fused_computation.21 | convolution fusion | flops 504496128 | bytes 5104640 | tf_op jit(solution)/shard_map/dot_general | solution.py:273
  270.4 2.4 reshape.225
  (71 shorter events, 15.6 us)
Async XLA Ops:
  6.5 182.6 %copy-start = (bf16[1,768,2048]{2,1,0:T(8,128)(2,1)S(1)}, bf16[1,768,2048]{2,1,0:T(8,128)(2,1)}, u32[]{:S(2)}) copy-start(bf16[1,768,2048]{2,1,0:T(8,128)(2,1)} %param.29) | copy-start | bytes 9437188
  6.5 107.6 %all-gather.2.cloned.1.call-start = ((), (), s32[]{:S(2)}) async-start(), calls=%async_computation.3 | async-start | bytes 4325376 | tf_op jit(solution)/shard_map/all_gather | solution.py:95
  56.8 5.7 %slice-start = ((bf16[192,4,2,192]{3,2,0,1:T(2,128)(2,1)}), bf16[192,4,2,64]{3,2,0,1:T(2,128)(2,1)S(1)}, s32[]{:S(2)}) async-start(bf16[192,4,2,192]{3,2,0,1:T(2,128)(2,1)} %reshape.216), calls=%async_computation.4 | async-start | bytes 786432 | tf_op jit(solution)/shard_map/slice | solution.py:214
  65.3 2.9 %copy-start.6 = (bf16[512,256]{1,0:T(8,128)(2,1)S(1)}, bf16[512,256]{1,0:T(8,128)(2,1)}, u32[]{:S(2)}) copy-start(bf16[512,256]{1,0:T(8,128)(2,1)} %param.20) | copy-start | bytes 786436
  65.3 2.9 %copy-start.9 = (f32[512]{0:T(512)S(1)}, f32[512]{0:T(512)}, u32[]{:S(2)}) copy-start(f32[512]{0:T(512)} %param.19) | copy-start | bytes 6148
  68.2 3.1 %slice-start.1 = ((bf16[192,4,2,192]{3,2,0,1:T(2,128)(2,1)}), bf16[192,4,2,128]{3,2,0,1:T(2,128)(2,1)S(1)}, s32[]{:S(2)}) async-start(bf16[192,4,2,192]{3,2,0,1:T(2,128)(2,1)} %reshape.216), calls=%async_computation.5 | async-start | bytes 786432 | tf_op jit(solution)/shard_map/slice | solution.py:213
  71.3 1.1 copy-start.4
  73.5 1.4 copy-start.7
  79.1 8.8 %copy-start.10 = (s32[48,4,2]{0,2,1:T(2,128)S(1)}, s32[48,4,2]{0,2,1:T(2,128)}, u32[]{:S(2)}) copy-start(s32[48,4,2]{0,2,1:T(2,128)} %param.26) | copy-start | bytes 4612
  80.5 17.2 %all-to-all-start = ((bf16[192,4,256]{2,1,0:T(4,128)(2,1)}), bf16[192,4,256]{2,1,0:T(4,128)(2,1)S(1)}, u32[]{:S(2)}, u32[]{:S(2)}) async-start(bf16[192,4,256]{2,1,0:T(4,128)(2,1)} %reshape.231), calls=%async_computation | async-start | bytes 786432 | tf_op jit(solution)/shard_map/all_to_all | solution.py:236
  114.2 3.8 %copy-start.5 = (pred[192,640]{1,0:T(8,128)(4,1)S(1)}, pred[192,640]{1,0:T(8,128)(4,1)}, u32[]{:S(2)}) copy-start(pred[192,640]{1,0:T(8,128)(4,1)} %get-tuple-element.20) | copy-start | bytes 368644
  114.2 3.8 %copy-start.11 = (f32[2048]{0:T(1024)S(1)}, f32[2048]{0:T(1024)}, u32[]{:S(2)}) copy-start(f32[2048]{0:T(1024)} %param.23) | copy-start | bytes 24580
  118.0 66.1 %copy-start.1 = (f32[192,2048]{1,0:T(8,128)}, f32[192,2048]{1,0:T(8,128)S(1)}, u32[]{:S(2)}) copy-start(f32[192,2048]{1,0:T(8,128)S(1)} %get-tuple-element.26) | copy-start | bytes 4718596
  119.0 66.6 %copy-start.13 = (bf16[1,2048,768]{2,1,0:T(8,128)(2,1)S(1)}, bf16[1,2048,768]{2,1,0:T(8,128)(2,1)}, u32[]{:S(2)}) copy-start(bf16[1,2048,768]{2,1,0:T(8,128)(2,1)} %param.27) | copy-start | bytes 9437188
  184.1 1.5 copy-start.2
  198.7 4.6 %copy-start.8 = (f32[48,4,2]{0,2,1:T(2,128)S(1)}, f32[48,4,2]{0,2,1:T(2,128)}, u32[]{:S(2)}) copy-start(f32[48,4,2]{0,2,1:T(2,128)} %param.25) | copy-start | bytes 4612
  198.7 4.8 %copy-start.12 = (f32[48,4]{0,1:T(4,128)S(1)}, f32[48,4]{0,1:T(4,128)}, u32[]{:S(2)}) copy-start(f32[48,4]{0,1:T(4,128)} %param.24) | copy-start | bytes 2308
  198.7 65.2 %copy-start.3 = (pred[192,2,640]{2,0,1:T(32,128)(4,1)S(1)}, pred[192,2,640]{2,0,1:T(32,128)(4,1)}, u32[]{:S(2)}) copy-start(pred[192,2,640]{2,0,1:T(32,128)(4,1)} %get-tuple-element.19) | copy-start | bytes 737284
  198.7 65.2 %all-to-all-start.2 = ((bf16[16,40,2048]{2,1,0:T(8,128)(2,1)}), bf16[16,40,2048]{2,1,0:T(8,128)(2,1)}, u32[]{:S(2)}, u32[]{:S(2)}) async-start(bf16[16,40,2048]{2,1,0:T(8,128)(2,1)} %bitcast.74), calls=%async_computation.2 | async-start | bytes 5242880 | tf_op jit(solution)/shard_map/all_to_all | solution.py:269
Sparse Core Ops, SparseCore 0:
  51.7 62.4 all-gather.1
